TPU v7x, 32 devices: a whole 2x2x4 slice. The times are simulated.
32 devices in a mesh: kv: 8 (over z, core), tp: 4 (over y, x).
Axes of the slice: x: 2, y: 2, z: 4, core: 2. Of those that a mesh axis runs over, the one named last changes fastest.
Arguments:
- tokens: bfloat16 [16, 2048], P(None, 'kv'), may hold values from -8 to 8
- lengths: int32 [16], replicated, may hold values from 1 to 3072, 12288 in all
- latent_cache: bfloat16 [16, 3072, 256], P(None, ('kv', 'tp')), may hold values from -10 to 10
- rope_cache: bfloat16 [16, 3072, 32], P(None, ('kv', 'tp')), may hold values from -2000 to 2000
- gain_in: bfloat16 [2048], P('kv'), may hold values from 0.099609375 to 1.8984375
- w_down_q: bfloat16 [2048, 512], P('kv'), may hold values from -0.125 to 0.125
- w_down_kv: bfloat16 [2048, 256], P('kv'), may hold values from -0.125 to 0.125
- w_rope_key: bfloat16 [2048, 32], P('kv'), may hold values from -0.125 to 0.125
- gain_q: bfloat16 [512], replicated, may hold values from 0.099609375 to 1.8984375
- w_up_qn: bfloat16 [512, 16, 64], replicated, may hold values from -0.25 to 0.25
- w_up_qr: bfloat16 [512, 16, 32], replicated, may hold values from -0.25 to 0.25
- gain_kv: bfloat16 [256], replicated, may hold values from 0.099609375 to 1.8984375
- w_key_up: bfloat16 [256, 16, 64], replicated, may hold values from -0.375 to 0.375
- w_value_up: bfloat16 [256, 16, 64], replicated, may hold values from -0.375 to 0.375
- w_attn_out: bfloat16 [16, 64, 2048], P('tp', None, 'kv'), may hold values from -0.1875 to 0.1875
- gain_mid: bfloat16 [2048], P('kv'), may hold values from 0.099609375 to 1.8984375
- w_ff_in: bfloat16 [2048, 8192], P('kv', 'tp'), may hold values from -0.125 to 0.125
- w_ff_out: bfloat16 [8192, 2048], P('tp', 'kv'), may hold values from -0.0625 to 0.0625
Outputs:
- mixed: bfloat16 [16, 2048], P(None, 'kv')
- new_latent: bfloat16 [16, 256], replicated
- new_rope_key: bfloat16 [16, 32], replicated
Inputs may be any that keep to these rules, and one draw needn't show every extreme that they name: `lengths`: each sequence's live cache positions; one sequence fills the whole cache.
All inputs are finite; a program needn't handle non-finite values.
Results may differ from a plain program's by a relative error of at most 0.012.
Values sent between devices are 32-bit elements; how exact they have to be, the bound alone decides.
A program may use at most 64 MiB of HBM per device.

v0:
```python
import jax
import jax.numpy as jnp
from jax import lax
from jax.sharding import PartitionSpec as P

D = 2048
NOPE = 64
ROPE = 32


EPS = 1e-06


def combined_all(part, axis, combine):
    gathered = jax.tree.map(lambda a: lax.all_gather(a, axis), part)

    def take(source):
        return jax.tree.map(lambda a: lax.dynamic_index_in_dim(a, source, 0, False), gathered)

    return lax.fori_loop(
        1, lax.axis_size(axis), lambda source, state: combine(state, take(source)), take(0)
    )


def rotate(values, positions):
    half = values.shape[-1] // 2
    inverse = 10000.0 ** (-jnp.arange(half, dtype=jnp.float32) / half)
    angle = positions.astype(jnp.float32)[:, None, None] * inverse[None, None, :]
    first = values[..., :half]
    second = values[..., half:]
    return jnp.concatenate(
        [
            first * jnp.cos(angle) - second * jnp.sin(angle),
            second * jnp.cos(angle) + first * jnp.sin(angle),
        ],
        axis=-1,
    )


def rms_scaled(values, gain):
    return (
        values
        * lax.rsqrt(jnp.mean(values * values, axis=-1, keepdims=True) + EPS)
        * gain.astype(jnp.float32)
    )


def combine(earlier, later):
    top_a, total_a, acc_a = earlier
    top_b, total_b, acc_b = later
    top = jnp.maximum(top_a, top_b)
    fade_a = jnp.exp(top_a - top)
    fade_b = jnp.exp(top_b - top)
    return (
        top,
        total_a * fade_a + total_b * fade_b,
        acc_a * fade_a[..., None] + acc_b * fade_b[..., None],
    )


def fold_sources(parts):
    tops, totals, accs = parts
    top = jnp.max(tops, axis=0)
    fade = jnp.exp(tops - top[None])
    return (top, jnp.sum(totals * fade, axis=0), jnp.sum(accs * fade[..., None], axis=0))


def per_device(
    tokens,
    lengths,
    latent_cache,
    rope_cache,
    gain_in,
    w_down_q,
    w_down_kv,
    w_rope_key,
    gain_q,
    w_up_qn,
    w_up_qr,
    gain_kv,
    w_key_up,
    w_value_up,
    w_attn_out,
    gain_mid,
    w_ff_in,
    w_ff_out,
):
    f32 = jnp.float32
    bf16 = jnp.bfloat16
    highest = lax.Precision.HIGHEST
    scale = (NOPE + ROPE) ** (-0.5)
    resid = tokens.astype(f32)
    scaled_in = (resid * gain_in.astype(f32)).astype(bf16)
    part_q = jnp.dot(scaled_in, w_down_q, preferred_element_type=f32)
    part_kv = jnp.dot(scaled_in, w_down_kv, preferred_element_type=f32)
    part_rope = jnp.dot(scaled_in, w_rope_key, preferred_element_type=f32)
    square_in = jnp.sum(resid * resid, axis=1)
    sum_q, sum_kv, sum_rope, total_in = lax.psum((part_q, part_kv, part_rope, square_in), "kv")
    inv_in = lax.rsqrt(total_in / D + EPS)[:, None]
    query_latent = rms_scaled(inv_in * sum_q, gain_q).astype(bf16)
    new_latent = rms_scaled(inv_in * sum_kv, gain_kv).astype(bf16)
    new_rope_key = rotate((inv_in * sum_rope)[:, None, :], lengths)[:, 0, :].astype(bf16)
    query_nope = jnp.einsum(
        "bc,chd->bhd", query_latent, w_up_qn, preferred_element_type=f32
    ).astype(bf16)
    query_rope = rotate(
        jnp.einsum("bc,chr->bhr", query_latent, w_up_qr, preferred_element_type=f32), lengths
    ).astype(bf16)
    query_cache = jnp.einsum(
        "bhd,khd->bhk", query_nope, w_key_up, preferred_element_type=f32
    ).astype(bf16)
    rows = latent_cache.shape[1]
    positions = lax.axis_index(("kv", "tp")) * rows + jnp.arange(rows, dtype=jnp.int32)
    live = (positions[None, :] < lengths[:, None])[:, None, :]
    scores = (
        jnp.einsum("bhk,blk->bhl", query_cache, latent_cache, preferred_element_type=f32)
        + jnp.einsum("bhr,blr->bhl", query_rope, rope_cache, preferred_element_type=f32)
    ) * scale
    scores = jnp.where(live, scores, -1e30)
    top = jnp.max(scores, axis=2)
    weights = jnp.where(live, jnp.exp(scores - top[:, :, None]), 0.0)
    total = jnp.sum(weights, axis=2)
    acc = jnp.einsum("bhl,blk->bhk", weights.astype(bf16), latent_cache, preferred_element_type=f32)
    heads_dev = w_attn_out.shape[0]
    first_head = lax.axis_index("tp") * heads_dev
    own_value_up = lax.dynamic_slice_in_dim(w_value_up, first_head, heads_dev, 1).astype(f32)
    own_cache_q = lax.dynamic_slice_in_dim(query_cache, first_head, heads_dev, 1)
    own_rope_q = lax.dynamic_slice_in_dim(query_rope, first_head, heads_dev, 1)
    self_score = (
        jnp.einsum("bhk,bk->bh", own_cache_q, new_latent, preferred_element_type=f32)
        + jnp.einsum("bhr,br->bh", own_rope_q, new_rope_key, preferred_element_type=f32)
    ) * scale
    top, total, acc = fold_sources(
        (
            lax.all_to_all(top[None], "tp", split_axis=2, concat_axis=0, tiled=True),
            lax.all_to_all(total[None], "tp", split_axis=2, concat_axis=0, tiled=True),
            lax.all_to_all(acc[None], "tp", split_axis=2, concat_axis=0, tiled=True),
        )
    )
    top, total, acc = combined_all((top, total, acc), "kv", combine)
    joined = jnp.maximum(top, self_score)
    fade = jnp.exp(top - joined)
    self_weight = jnp.exp(self_score - joined)
    total = total * fade + self_weight
    acc = (
        acc * fade[:, :, None]
        + self_weight.astype(bf16).astype(f32)[:, :, None] * new_latent.astype(f32)[:, None, :]
    )
    expanded = jnp.einsum("bhk,khv->bhv", acc, own_value_up, precision=highest)
    head_out = (expanded / total[:, :, None]).astype(bf16)
    attn_part = jnp.einsum("bhv,hvd->bd", head_out, w_attn_out, preferred_element_type=f32)
    resid_mid = resid + lax.psum(attn_part, "tp")
    scaled_mid = (resid_mid * gain_mid.astype(f32)).astype(bf16)
    hidden_part = jnp.dot(scaled_mid, w_ff_in, preferred_element_type=f32)
    square_mid = jnp.sum(resid_mid * resid_mid, axis=1)
    hidden_sum, total_mid = lax.psum((hidden_part, square_mid), "kv")
    inv_mid = lax.rsqrt(total_mid / D + EPS)[:, None]
    hidden = jnp.square(jax.nn.relu(inv_mid * hidden_sum)).astype(bf16)
    out_part = jnp.dot(hidden, w_ff_out, preferred_element_type=f32)
    mixed = (resid_mid + lax.psum(out_part, "tp")).astype(bf16)
    return (mixed, new_latent, new_rope_key)


def solution(mesh):
    return jax.shard_map(
        per_device,
        mesh=mesh,
        in_specs=(
            P(None, "kv"),
            P(),
            P(None, ("kv", "tp"), None),
            P(None, ("kv", "tp"), None),
            P("kv"),
            P("kv", None),
            P("kv", None),
            P("kv", None),
            P(),
            P(),
            P(),
            P(),
            P(),
            P(),
            P("tp", None, "kv"),
            P("kv"),
            P("kv", "tp"),
            P("tp", "kv"),
        ),
        out_specs=(P(None, "kv"), P(), P()),
        check_vma=False,
    )
```

profile of v0, /device:TPU:0, one launch (start us, length us, event | category | flops | bytes accessed | tf_op | source)
XLA Modules:
  0.0 218.2 jit_solution(16655276583001931939)
XLA Ops:
  7.2 0.8 convert_element_type.75
  8.0 0.8 fusion.23
  8.8 0.7 convert_element_type.68
  9.5 0.7 broadcast_compare_fusion
  10.2 0.7 convert_element_type.70
  10.9 0.9 fusion.41
  11.7 1.1 fusion.43
  12.8 1.2 fusion.45
  14.0 30.8 %all-reduce = (f32[16,512]{1,0:T(8,128)S(1)}, f32[16]{0:T(128)S(1)}, f32[16,256]{1,0:T(8,128)S(1)}, f32[16,32]{1,0:T(8,128)S(1)}) all-reduce(f32[16,512]{1,0:T(8,128)S(1)} %fusion.45, f32[16]{0:T(128)S(1)} %fusion.23, f32[16,256]{1,0:T(8,128)S(1)} %fusion.43, f32[16,32]{1,0:T(8,128)S(1)} %fusion.41), channel_id=1, replica_groups=mesh['kv'=8,'tp'=4] {'kv'}, use_global_device_ids=true, to_apply=%region_2.0 | all-reduce | flops 12816 | bytes 102528 | tf_op jit(solution)/shard_map/psum | solution.py:98
  44.8 0.2 multiply_reduce_fusion.1
  45.1 0.5 fusion.55
  45.6 0.7 convolution_convert_fusion
  46.5 0.1 fusion.14
  46.7 0.8 copy-done.1
  47.4 0.4 fusion.62
  47.8 0.7 copy.50
  48.5 3.7 %all-to-all-start = ((f32[1,16,16]{1,0,2:T(1,128)}), f32[1,16,16]{1,0,2:T(1,128)S(1)}, u32[]{:S(2)}, u32[]{:S(2)}) async-start(f32[1,16,16]{1,0,2:T(1,128)} %copy.50), calls=%async_computation | async-start | bytes 16384 | tf_op jit(solution)/shard_map/all_to_all | solution.py:135
  52.3 0.6 copy-done.10
  53.1 0.2 multiply_reduce_fusion.3
  53.3 0.3 convolution_bitcast_fusion
  53.6 0.7 fusion.52
  54.5 0.5 copy-done.9
  55.0 0.2 fusion.10
  55.3 0.6 copy-done.11
  56.1 0.7 copy.51
  56.8 0.8 copy.52
  57.6 4.2 %all-to-all-start.1 = ((f32[1,16,16]{1,0,2:T(1,128)}), f32[1,16,16]{1,0,2:T(1,128)S(1)}, u32[]{:S(2)}, u32[]{:S(2)}) async-start(f32[1,16,16]{1,0,2:T(1,128)} %copy.51), calls=%async_computation.1 | async-start | bytes 16384 | tf_op jit(solution)/shard_map/all_to_all | solution.py:136
  61.8 12.8 %all-gather.3 = f32[8,16,4]{1,2,0:T(4,128)S(1)} all-gather(f32[1,16,4]{1,2,0:T(4,128)S(1)} %bitcast.113), channel_id=2, replica_groups=mesh['kv'=8,'tp'=4] {'kv'}, dimensions={0}, use_global_device_ids=true | all-gather | bytes 2304 | tf_op jit(solution)/shard_map/all_gather | solution.py:15
  74.6 4.2 %all-to-all-start.2 = ((f32[1,16,16,256]{3,1,0,2:T(8,128)}), f32[1,16,16,256]{3,1,0,2:T(8,128)S(1)}, u32[]{:S(2)}, u32[]{:S(2)}) async-start(f32[1,16,16,256]{3,1,0,2:T(8,128)} %copy.52), calls=%async_computation.2 | async-start | bytes 524288 | tf_op jit(solution)/shard_map/all_to_all | solution.py:137
  78.8 12.8 %all-gather.4 = f32[8,16,4]{1,2,0:T(4,128)S(1)} all-gather(f32[1,16,4]{1,2,0:T(4,128)S(1)} %bitcast.114), channel_id=3, replica_groups=mesh['kv'=8,'tp'=4] {'kv'}, dimensions={0}, use_global_device_ids=true | all-gather | bytes 2304 | tf_op jit(solution)/shard_map/all_gather | solution.py:15
  91.8 15.1 %all-gather.2 = f32[128,4,256]{2,1,0:T(4,128)S(1)} all-gather(f32[16,4,256]{2,1,0:T(4,128)S(1)} %copy.53), channel_id=4, replica_groups=mesh['kv'=8,'tp'=4] {'kv'}, dimensions={0}, use_global_device_ids=true | all-gather | bytes 589824 | tf_op jit(solution)/shard_map/all_gather | solution.py:15
  106.8 2.5 %while.19 = (s32[]{:T(128)}, f32[16,4]{0,1:T(4,128)S(1)}, f32[16,4]{0,1:T(4,128)S(1)}, f32[16,4,256]{2,1,0:T(4,128)S(1)}, f32[8,16,4]{1,2,0:T(4,128)S(1)}, /*ind...) while((s32[]{:T(128)}, f32[16,4]{0,1:T(4,128)S(1)}, ...), condition=%wide.region_10.11_spmd, body=%wide.region_9.10_spmd.sunk | while | flops 49541 | bytes 200335 | solution.py:20
  107.0 0.1 fusion.79
  107.4 0.1 fusion.79
  107.8 0.1 fusion.79
  108.1 0.1 fusion.79
  108.5 0.1 fusion.79
  108.8 0.1 fusion.79
  109.2 0.1 fusion.79
  109.6 1.2 fusion.6
  110.8 0.2 convolution_bitcast_fusion.2
  111.0 16.5 %psum.60 = f32[16,256]{1,0:T(8,128)S(1)} all-reduce(f32[16,256]{1,0:T(8,128)S(1)} %convolution_bitcast_fusion.2), channel_id=1, replica_groups=mesh['kv'=8,'tp'=4] {'tp'}, use_global_device_ids=true, to_apply=%region_14.15 | all-reduce | flops 4096 | bytes 32768 | tf_op jit(solution)/shard_map/psum | solution.py:152
  127.6 13.6 %psum.61 = f32[16]{0:T(128)S(1)} all-reduce(f32[16]{0:T(128)S(1)} %multiply_reduce_fusion.2), channel_id=1, replica_groups=mesh['kv'=8,'tp'=4] {'kv'}, use_global_device_ids=true, to_apply=%region_16.17 | all-reduce | flops 16 | bytes 128 | tf_op jit(solution)/shard_map/psum | solution.py:156
  141.2 0.9 fusion.38
  142.2 51.4 %all-reduce.3.cloned.1.call-done = f32[16,2048]{1,0:T(8,128)} async-done(((f32[16,2048]{1,0:T(8,128)}), f32[16,2048]{1,0:T(8,128)}) %all-reduce.3.cloned.1.call-update) | async-done | bytes 131088 | tf_op jit(solution)/shard_map/psum | solution.py:156
  193.6 1.2 fusion.12
  194.8 16.0 %psum.63 = f32[16,256]{1,0:T(8,128)S(1)} all-reduce(f32[16,256]{1,0:T(8,128)S(1)} %fusion.12), channel_id=1, replica_groups=mesh['kv'=8,'tp'=4] {'tp'}, use_global_device_ids=true, to_apply=%region_18.19 | all-reduce | flops 4096 | bytes 32768 | tf_op jit(solution)/shard_map/psum | solution.py:160
  210.7 0.6 add_convert_fusion.1
  (78 shorter events, 3.2 us)
Async XLA Ops:
  7.2 38.4 %copy-start = (bf16[512,16,64]{0,2,1:T(8,128)(2,1)S(1)}, bf16[512,16,64]{0,2,1:T(8,128)(2,1)}, u32[]{:S(2)}) copy-start(bf16[512,16,64]{0,2,1:T(8,128)(2,1)} %param.29) | copy-start | bytes 3145732
  7.2 37.9 %copy-start.4 = (bf16[512,16,32]{0,2,1:T(8,128)(2,1)S(1)}, bf16[512,16,32]{0,2,1:T(8,128)(2,1)}, u32[]{:S(2)}) copy-start(bf16[512,16,32]{0,2,1:T(8,128)(2,1)} %param.30) | copy-start | bytes 1572868
  12.8 32.8 %copy-start.5 = (bf16[256,16,64]{0,2,1:T(8,128)(2,1)S(1)}, bf16[256,16,64]{0,2,1:T(8,128)(2,1)}, u32[]{:S(2)}) copy-start(bf16[256,16,64]{0,2,1:T(8,128)(2,1)} %param.32) | copy-start | bytes 1572868
  45.6 0.9 copy-start.8
  46.3 1.2 copy-start.1
  48.5 9.1 %all-to-all-start = ((f32[1,16,16]{1,0,2:T(1,128)}), f32[1,16,16]{1,0,2:T(1,128)S(1)}, u32[]{:S(2)}, u32[]{:S(2)}) async-start(f32[1,16,16]{1,0,2:T(1,128)} %copy.50), calls=%async_computation | async-start | bytes 16384 | tf_op jit(solution)/shard_map/all_to_all | solution.py:135
  52.2 0.7 copy-start.10
  54.3 0.6 copy-start.9
  55.3 0.7 copy-start.11
  57.6 17.0 %all-to-all-start.1 = ((f32[1,16,16]{1,0,2:T(1,128)}), f32[1,16,16]{1,0,2:T(1,128)S(1)}, u32[]{:S(2)}, u32[]{:S(2)}) async-start(f32[1,16,16]{1,0,2:T(1,128)} %copy.51), calls=%async_computation.1 | async-start | bytes 16384 | tf_op jit(solution)/shard_map/all_to_all | solution.py:136
  74.6 17.0 %all-to-all-start.2 = ((f32[1,16,16,256]{3,1,0,2:T(8,128)}), f32[1,16,16,256]{3,1,0,2:T(8,128)S(1)}, u32[]{:S(2)}, u32[]{:S(2)}) async-start(f32[1,16,16,256]{3,1,0,2:T(8,128)} %copy.52), calls=%async_computation.2 | async-start | bytes 524288 | tf_op jit(solution)/shard_map/all_to_all | solution.py:137
  78.8 114.8 %all-reduce.3.cloned.1.call-start = ((), (), s32[]{:S(2)}) async-start(), calls=%async_computation.3 | async-start | bytes 262144 | tf_op jit(solution)/shard_map/psum | solution.py:156
  91.7 19.0 %copy-start.7 = (bf16[4,64,256]{2,1,0:T(8,128)(2,1)S(1)}, bf16[4,64,256]{2,1,0:T(8,128)(2,1)}, u32[]{:S(2)}) copy-start(bf16[4,64,256]{2,1,0:T(8,128)(2,1)} %param.34) | copy-start | bytes 393220
  106.8 34.4 %copy-start.2 = (bf16[256,2048]{1,0:T(8,128)(2,1)S(1)}, bf16[256,2048]{1,0:T(8,128)(2,1)}, u32[]{:S(2)}) copy-start(bf16[256,2048]{1,0:T(8,128)(2,1)} %param.36) | copy-start | bytes 3145732
  106.8 20.7 %copy-start.6 = (bf16[16,256]{1,0:T(8,128)(2,1)S(1)}, bf16[16,256]{1,0:T(8,128)(2,1)}, u32[]{:S(2)}) copy-start(bf16[16,256]{1,0:T(8,128)(2,1)} %param.20) | copy-start | bytes 24580
  109.3 84.3 %copy-start.3 = (bf16[2048,256]{1,0:T(8,128)(2,1)S(1)}, bf16[2048,256]{1,0:T(8,128)(2,1)}, u32[]{:S(2)}) copy-start(bf16[2048,256]{1,0:T(8,128)(2,1)} %param.37) | copy-start | bytes 3145732
Sparse Core Ops, SparseCore 0:
  142.3 51.2 all-reduce.2
where the time goes:
time: 219 us; the launch traced here: 218 us
  blocking collectives  117 us (53%)
  waiting for transfers between devices  51.5 us (24%)
  between operations  14.2 us (6%)
  starting transfers between devices  12.1 us (6%)
  matrix products  8.74 us (4%)
  other arithmetic  7.81 us (4%)
  local copies, waits for them, and re-layouts  6.26 us (3%)
    psum x1, waiting for transfers between devices, per_device(): hidden_sum, total_mid = lax.psum((hidden_part, square_mid), 'kv')  51.4 us
    all_gather x3, blocking collectives, combined_all(): gathered = jax.tree.map(lambda a: lax.all_gather(a, axis), part)  40.6 us
    psum x1, blocking collectives, per_device(): lax.psum((part_q, part_kv, part_rope, square_in), 'kv')  30.8 us
    psum x1, blocking collectives, per_device(): resid_mid = resid + lax.psum(attn_part, 'tp')  16.5 us
    psum x1, blocking collectives, per_device(): mixed = (resid_mid + lax.psum(out_part, 'tp')).astype(bf16)  16 us
    psum x1, blocking collectives, per_device(): hidden_sum, total_mid = lax.psum((hidden_part, square_mid), 'kv')  13.6 us
  transfers between devices with their start and end apart: 4, of which 1 were waited for; matrix products, arithmetic and copies ran while one was open for 2% of the time, Pallas kernels for 0%

commit v1 on v0

--- a/solution.py
+++ b/solution.py
@@ -1,6 +1,10 @@
+import functools
+
 import jax
 import jax.numpy as jnp
 from jax import lax
+from jax.experimental import pallas as pl
+from jax.experimental.pallas import tpu as pltpu
 from jax.sharding import PartitionSpec as P
 
 D = 2048
@@ -160,10 +164,397 @@
     mixed = (resid_mid + lax.psum(out_part, "tp")).astype(bf16)
     return (mixed, new_latent, new_rope_key)
 
+MESH = pl.DeviceIdType.MESH
+LANES = 128
+
+
+def dot_nt(a, b):
+    return lax.dot_general(a, b, (((1,), (1,)), ((), ())), preferred_element_type=jnp.float32)
+
+
+def dot_nn(a, b):
+    return jnp.dot(a, b, preferred_element_type=jnp.float32)
+
+
+def turn(values, cos, sin, half):
+    width = values.shape[1]
+    lane = lax.broadcasted_iota(jnp.int32, values.shape, 1)
+    partner = jnp.where(
+        lane % (2 * half) < half,
+        -pltpu.roll(values, width - half, 1),
+        pltpu.roll(values, half, 1),
+    )
+    return values * cos + partner * sin
+
+
+def layer_kernel(
+    n_kv, n_tp,
+    tokens, lengths, gain_in, gain_q, gain_kv, gain_mid,
+    latent_h, rope_h, down_q_h, down_kv_h, down_r_h, up_qn_h, up_qr_h, key_up_h, value_up_h,
+    attn_out_h, ff_in_h, ff_out_h,
+    mixed_ref, new_latent_ref, new_rope_ref,
+    latent, rope, down_q, down_kv, down_r, up_qn, up_qr, key_up, value_up, attn_out, ff_in, ff_out,
+    part_in, got_in, full_in, q_rows, r_rows, acc_rows, part_att, got_att, head_rows,
+    part_out, got_out, part_stat, got_stat, part_ff, got_ff, full_ff, part_mix, got_mix,
+    load_sem, send_sem, recv_sem,
+):
+    f32 = jnp.float32
+    bf16 = jnp.bfloat16
+    kv = lax.axis_index("kv")
+    tp = lax.axis_index("tp")
+    n_all = n_kv * n_tp
+    me = kv * n_tp + tp
+    loads = []
+    for i, (src, dst) in enumerate((
+        (down_q_h, down_q), (down_kv_h, down_kv), (down_r_h, down_r), (up_qn_h, up_qn),
+        (up_qr_h, up_qr), (key_up_h, key_up), (latent_h, latent), (rope_h, rope),
+        (value_up_h, value_up), (attn_out_h, attn_out), (ff_in_h, ff_in), (ff_out_h, ff_out),
+    )):
+        copy = pltpu.make_async_copy(src, dst, load_sem.at[i])
+        copy.start()
+        loads.append(copy)
+
+    barrier = pltpu.get_barrier_semaphore()
+    for d in range(1, n_all):
+        peer = lax.rem(me + d, n_all)
+        pl.semaphore_signal(
+            barrier, inc=1, device_id=(peer // n_tp, lax.rem(peer, n_tp)), device_id_type=MESH
+        )
+
+    def remote(src, dst, slot, where):
+        return pltpu.make_async_remote_copy(
+            src_ref=src, dst_ref=dst, send_sem=send_sem.at[slot], recv_sem=recv_sem.at[slot],
+            device_id=where, device_id_type=MESH,
+        )
+
+    sent = []
+    slots = [0]
+
+    def begin(axis, src_of, dst_of):
+        count, mine = {"kv": (n_kv, kv), "tp": (n_tp, tp), "all": (n_all, me)}[axis]
+        base = slots[0]
+        slots[0] += count - 1
+
+        def where(index):
+            if axis == "kv":
+                return (index, tp)
+            if axis == "tp":
+                return (kv, index)
+            return (index // n_tp, lax.rem(index, n_tp))
+
+        arriving = []
+        for d in range(1, count):
+            peer = lax.rem(mine + d, count)
+            copy = remote(src_of(peer), dst_of(mine), base + d - 1, where(peer))
+            copy.start()
+            sent.append(copy)
+            source = lax.rem(mine + count - d, count)
+            arriving.append(remote(dst_of(source), dst_of(source), base + d - 1, where(source)))
+
+        def finish():
+            for copy in arriving:
+                copy.wait_recv()
+
+        return finish
+
+    seqs, width = tokens.shape
+    q_rank = down_q.shape[1]
+    kv_rank = down_kv.shape[1]
+    rope_size = down_r.shape[0]
+    half = rope_size // 2
+    heads = key_up.shape[0]
+    nope = key_up.shape[1]
+    v_size = value_up.shape[1]
+    rows = latent.shape[1]
+    own_heads = heads // n_tp
+    own_seqs = seqs // n_kv
+    scale = (nope + rope_size) ** (-0.5)
+    d_model = width * n_kv
+
+    resid = tokens[...].astype(f32)
+    scaled_in = (resid * gain_in[...].astype(f32)).astype(bf16)
+    for copy in loads[:3]:
+        copy.wait()
+    square = jnp.sum(resid * resid, axis=1, keepdims=True)
+    part = jnp.concatenate(
+        [
+            dot_nn(scaled_in, down_q[...]),
+            dot_nn(scaled_in, down_kv[...]),
+            dot_nt(scaled_in, down_r[...]),
+            jnp.zeros((seqs, LANES - rope_size), f32),
+            jnp.broadcast_to(square, (seqs, LANES)),
+        ],
+        axis=1,
+    )
+    block = part.shape[1] // n_tp
+    for i in range(n_tp):
+        part_in[i] = part[:, i * block : (i + 1) * block]
+    pl.semaphore_wait(barrier, n_all - 1)
+    finish = begin("kv", lambda k: part_in.at[tp], lambda k: got_in.at[k])
+    got_in[kv] = part_in[tp]
+
+    lane = lax.broadcasted_iota(jnp.int32, (seqs, LANES), 1)
+    row = lax.broadcasted_iota(jnp.int32, (seqs, LANES), 0)
+    where_at = jnp.zeros((seqs, LANES), jnp.int32)
+    for b in range(seqs):
+        where_at = jnp.where(row == b, lengths[b], where_at)
+    inverse = jnp.zeros((seqs, LANES), f32)
+    for j in range(half):
+        inverse = jnp.where(lane % half == j, 10000.0 ** (-j / half), inverse)
+    angle = where_at.astype(f32) * inverse
+    cos, sin = jnp.cos(angle), jnp.sin(angle)
+    finish()
+    full_in[tp] = jnp.sum(got_in[...], axis=0)
+    finish = begin("tp", lambda t: full_in.at[tp], lambda t: full_in.at[t])
+    for copy in loads[3:6]:
+        copy.wait()
+    finish()
+    sums = jnp.concatenate([full_in[i] for i in range(n_tp)], axis=1)
+    inv_in = lax.rsqrt(sums[:, q_rank + kv_rank + LANES :][:, :1] / d_model + EPS)
+    lat_q = inv_in * sums[:, :q_rank]
+    query_latent = (
+        lat_q
+        * lax.rsqrt(jnp.mean(lat_q * lat_q, axis=1, keepdims=True) + EPS)
+        * gain_q[...].astype(f32)
+    ).astype(bf16)
+    lat_kv = inv_in * sums[:, q_rank : q_rank + kv_rank]
+    new_latent = (
+        lat_kv
+        * lax.rsqrt(jnp.mean(lat_kv * lat_kv, axis=1, keepdims=True) + EPS)
+        * gain_kv[...].astype(f32)
+    ).astype(bf16)
+    new_latent_ref[...] = new_latent
+    new_latent = new_latent.astype(f32)
+    new_rope = turn(
+        inv_in * sums[:, q_rank + kv_rank : q_rank + kv_rank + LANES], cos, sin, half
+    ).astype(bf16)
+    new_rope_ref[...] = new_rope[:, :rope_size]
+    new_rope = new_rope.astype(f32)[:, :rope_size]
+
+    query_nope = dot_nt(query_latent, up_qn[...]).astype(bf16)
+    times = heads * rope_size // LANES
+    query_rope = turn(
+        dot_nt(query_latent, up_qr[...]),
+        jnp.concatenate([cos] * times, axis=1),
+        jnp.concatenate([sin] * times, axis=1),
+        half,
+    ).astype(bf16).astype(f32)
+    for h in range(heads):
+        q_rows[h] = dot_nn(query_nope[:, h * nope : (h + 1) * nope], key_up[h]).astype(
+            bf16
+        ).astype(f32)
+        r_rows[h] = query_rope[:, h * rope_size : (h + 1) * rope_size]
+
+    for copy in loads[6:9]:
+        copy.wait()
+    first = me * rows
+    at = first + lax.broadcasted_iota(jnp.int32, (heads, rows), 1)
+    scores, selfs, lives = [], [], []
+    for b in range(seqs):
+        q_b = q_rows[:, b, :]
+        r_b = r_rows[:, b, :]
+        score = (
+            dot_nt(q_b.astype(bf16), latent[b]) + dot_nn(r_b.astype(bf16), rope[b])
+        ) * scale
+        live = at < lengths[b]
+        scores.append(jnp.where(live, score, -1e30))
+        lives.append(live)
+        own = (
+            jnp.sum(q_b * new_latent[b : b + 1, :], axis=1, keepdims=True)
+            + jnp.sum(r_b * new_rope[b : b + 1, :], axis=1, keepdims=True)
+        ) * scale
+        selfs.append(own)
+    mine = me == 0
+    for b in range(seqs):
+        own = jnp.where(mine, selfs[b], -1e30)
+        top = jnp.maximum(jnp.max(scores[b], axis=1, keepdims=True), own)
+        weights = jnp.where(lives[b], jnp.exp(scores[b] - top), 0.0)
+        own_weight = jnp.where(mine, jnp.exp(own - top), 0.0)
+        total = jnp.sum(weights, axis=1, keepdims=True) + own_weight
+        acc_rows[b, :, :kv_rank] = (
+            dot_nn(weights.astype(bf16), latent[b])
+            + own_weight.astype(bf16).astype(f32) * new_latent[b : b + 1, :]
+        )
+        acc_rows[b, :, kv_rank : kv_rank + LANES] = jnp.broadcast_to(top, (heads, LANES))
+        acc_rows[b, :, kv_rank + LANES :] = jnp.broadcast_to(total, (heads, LANES))
+
+    v_wide = own_heads * v_size
+    for t in range(n_tp):
+        pieces = []
+        stat = jnp.zeros((seqs, LANES), f32)
+        for i in range(own_heads):
+            h = t * own_heads + i
+            acc = acc_rows[:, h, :]
+            exact = acc[:, :kv_rank]
+            high = exact.astype(bf16)
+            low = (exact - high.astype(f32)).astype(bf16)
+            both = dot_nt(jnp.concatenate([high, low], axis=0), value_up[h])
+            pieces.append(both[:seqs] + both[seqs:])
+            stat = jnp.where(lane == i, acc[:, kv_rank : kv_rank + LANES], stat)
+            stat = jnp.where(lane == own_heads + i, acc[:, kv_rank + LANES :], stat)
+        message = jnp.concatenate(pieces + [stat], axis=1)
+        for k in range(n_kv):
+            part_att[k * n_tp + t] = message[k * own_seqs : (k + 1) * own_seqs, :]
+    finish = begin("all", lambda p: part_att.at[p], lambda p: got_att.at[p])
+    got_att[me] = part_att[me]
+    finish()
+    got = got_att[...]
+    values = got[:, :, :v_wide]
+    stat = got[:, :, v_wide:]
+    fade_all = jnp.exp(stat - jnp.max(stat, axis=0, keepdims=True))
+    head_lane = lax.broadcasted_iota(jnp.int32, values.shape, 2) // v_size
+    sum_lane = lax.broadcasted_iota(jnp.int32, (own_seqs, v_wide), 1) // v_size
+    fade = jnp.zeros(values.shape, f32)
+    total = jnp.ones((own_seqs, v_wide), f32)
+    for i in range(own_heads):
+        fade_i = fade_all[:, :, i : i + 1]
+        total_i = jnp.sum(stat[:, :, own_heads + i : own_heads + i + 1] * fade_i, axis=0)
+        fade = jnp.where(head_lane == i, fade_i, fade)
+        total = jnp.where(sum_lane == i, total_i, total)
+    head_rows[kv] = (jnp.sum(values * fade, axis=0) / total).astype(bf16).astype(f32)
+    finish = begin("kv", lambda k: head_rows.at[kv], lambda k: head_rows.at[k])
+    loads[9].wait()
+    finish()
+    head_out = jnp.concatenate([head_rows[k] for k in range(n_kv)], axis=0).astype(bf16)
+
+    got_out[tp] = dot_nn(head_out, attn_out[...])
+    finish = begin("tp", lambda t: got_out.at[tp], lambda t: got_out.at[t])
+    loads[10].wait()
+    finish()
+    resid_mid = resid + jnp.sum(got_out[...], axis=0)
+    got_stat[kv] = jnp.broadcast_to(
+        jnp.sum(resid_mid * resid_mid, axis=1, keepdims=True), (seqs, LANES)
+    )
+    finish_stat = begin("kv", lambda k: got_stat.at[kv], lambda k: got_stat.at[k])
+    scaled_mid = (resid_mid * gain_mid[...].astype(f32)).astype(bf16)
+    hidden_part = dot_nn(scaled_mid, ff_in[...])
+    piece = hidden_part.shape[1] // n_kv
+    for k in range(n_kv):
+        part_ff[k] = hidden_part[:, k * piece : (k + 1) * piece]
+    finish = begin("kv", lambda k: part_ff.at[k], lambda k: got_ff.at[k])
+    got_ff[kv] = part_ff[kv]
+    finish_stat()
+    inv_mid = lax.rsqrt(jnp.sum(got_stat[...], axis=0)[:, :1] / d_model + EPS)
+    loads[11].wait()
+    finish()
+    full_ff[kv] = jnp.sum(got_ff[...], axis=0)
+    finish = begin("kv", lambda k: full_ff.at[kv], lambda k: full_ff.at[k])
+    finish()
+    hidden_sum = jnp.concatenate([full_ff[k] for k in range(n_kv)], axis=1)
+    hidden = jnp.square(jnp.maximum(inv_mid * hidden_sum, 0.0)).astype(bf16)
+    got_mix[tp] = dot_nn(hidden, ff_out[...])
+    finish = begin("tp", lambda t: got_mix.at[tp], lambda t: got_mix.at[t])
+    finish()
+    mixed_ref[...] = (resid_mid + jnp.sum(got_mix[...], axis=0)).astype(bf16)
+    for copy in sent:
+        copy.wait_send()
+
+
+def per_device_kernel(
+    n_kv, n_tp,
+    tokens, lengths, latent_cache, rope_cache, gain_in, w_down_q, w_down_kv, w_rope_key, gain_q,
+    w_up_qn, w_up_qr, gain_kv, w_key_up, w_value_up, w_attn_out, gain_mid, w_ff_in, w_ff_out,
+):
+    f32 = jnp.float32
+    bf16 = jnp.bfloat16
+    seqs, width = tokens.shape
+    q_rank, heads, nope = w_up_qn.shape
+    kv_rank, _, v_size = w_value_up.shape
+    rope_size = w_rope_key.shape[1]
+    hidden = w_ff_in.shape[1]
+    n_all = n_kv * n_tp
+    own_seqs = seqs // n_kv
+    v_wide = heads // n_tp * v_size
+    big = [
+        latent_cache,
+        rope_cache.transpose(0, 2, 1),
+        w_down_q,
+        w_down_kv,
+        w_rope_key.T,
+        w_up_qn.transpose(1, 2, 0).reshape(heads * nope, q_rank),
+        w_up_qr.transpose(1, 2, 0).reshape(heads * rope_size, q_rank),
+        w_key_up.transpose(1, 2, 0),
+        w_value_up.transpose(1, 2, 0),
+        w_attn_out.reshape(-1, width),
+        w_ff_in,
+        w_ff_out,
+    ]
+    block = (q_rank + kv_rank + 2 * LANES) // n_tp
+    messages = 5 * (n_kv - 1) + 3 * (n_tp - 1) + (n_all - 1)
+    vmem = pltpu.VMEM
+    whole = pl.BlockSpec(memory_space=pltpu.VMEM)
+    return pl.pallas_call(
+        functools.partial(layer_kernel, n_kv, n_tp),
+        out_shape=(
+            jax.ShapeDtypeStruct((seqs, width), bf16),
+            jax.ShapeDtypeStruct((seqs, kv_rank), bf16),
+            jax.ShapeDtypeStruct((seqs, rope_size), bf16),
+        ),
+        in_specs=[whole, pl.BlockSpec(memory_space=pltpu.SMEM)]
+        + [whole] * 4
+        + [pl.BlockSpec(memory_space=pl.ANY)] * len(big),
+        out_specs=(whole, whole, whole),
+        scratch_shapes=[vmem(a.shape, bf16) for a in big]
+        + [
+            vmem((n_tp, seqs, block), f32),
+            vmem((n_kv, seqs, block), f32),
+            vmem((n_tp, seqs, block), f32),
+            vmem((heads, seqs, kv_rank), f32),
+            vmem((heads, seqs, rope_size), f32),
+            vmem((seqs, heads, kv_rank + 2 * LANES), f32),
+            vmem((n_all, own_seqs, v_wide + LANES), f32),
+            vmem((n_all, own_seqs, v_wide + LANES), f32),
+            vmem((n_kv, own_seqs, v_wide), f32),
+            vmem((8, LANES), f32),
+            vmem((n_tp, seqs, width), f32),
+            vmem((8, LANES), f32),
+            vmem((n_kv, seqs, LANES), f32),
+            vmem((n_kv, seqs, hidden // n_kv), f32),
+            vmem((n_kv, seqs, hidden // n_kv), f32),
+            vmem((n_kv, seqs, hidden // n_kv), f32),
+            vmem((8, LANES), f32),
+            vmem((n_tp, seqs, width), f32),
+            pltpu.SemaphoreType.DMA((len(big),)),
+            pltpu.SemaphoreType.DMA((messages,)),
+            pltpu.SemaphoreType.DMA((messages,)),
+        ],
+        compiler_params=pltpu.CompilerParams(collective_id=0, has_side_effects=True),
+        name="layer",
+    )(
+        tokens, lengths, gain_in.reshape(1, -1), gain_q.reshape(1, -1), gain_kv.reshape(1, -1),
+        gain_mid.reshape(1, -1), *big,
+    )
+
+
+def kernel_fits(n_kv, n_tp, seqs, width, q_rank, kv_rank, rope_size, heads, v_size, hidden):
+    return (
+        seqs % n_kv == 0
+        and heads % n_tp == 0
+        and width % LANES == 0
+        and q_rank % LANES == 0
+        and kv_rank % LANES == 0
+        and LANES % rope_size == 0
+        and (heads * rope_size) % LANES == 0
+        and (q_rank + kv_rank + 2 * LANES) % (n_tp * LANES) == 0
+        and (heads // n_tp * v_size) % LANES == 0
+        and hidden % (n_kv * LANES) == 0
+    )
+
+
+def per_device_any(n_kv, n_tp, *args):
+    tokens, w_down_q, w_down_kv, w_rope_key = args[0], args[5], args[6], args[7]
+    w_value_up, w_ff_in = args[13], args[16]
+    if kernel_fits(
+        n_kv, n_tp, *tokens.shape, w_down_q.shape[1], w_down_kv.shape[1], w_rope_key.shape[1],
+        *w_value_up.shape[1:], w_ff_in.shape[1],
+    ):
+        return per_device_kernel(n_kv, n_tp, *args)
+    return per_device(*args)
+
 
 def solution(mesh):
     return jax.shard_map(
-        per_device,
+        functools.partial(per_device_any, mesh.shape["kv"], mesh.shape["tp"]),
         mesh=mesh,
         in_specs=(
             P(None, "kv"),

time: 219 us -> 52 us (0.24)
  blocking collectives: 117 us -> 0 us
  waiting for transfers between devices: 51.5 us -> 0 us
  Pallas kernels: 0 us -> 45.2 us
  between operations: 14.2 us -> 0.66 us
  starting transfers between devices: 12.1 us -> 0 us
  matrix products: 8.74 us -> 0 us
  other arithmetic: 7.81 us -> 0 us
    psum x4 -> x0, blocking collectives: 76.9 us -> none  [the longest x1 30.8 us: per_device(): lax.psum((part_q, part_kv, part_rope, square_in), 'kv')]
    psum x1 -> x0, waiting for transfers between devices: 51.4 us -> none  [per_device(): hidden_sum, total_mid = lax.psum((hidden_part, square_mid), 'kv')]
    pallas_call x0 -> x1, Pallas kernels: none -> 45.2 us  [per_device_kernel(): pl.pallas_call(functools.partial(layer_kernel, n_kv, n_tp), out_shape=(ja...]
    all_gather x3 -> x0, blocking collectives: 40.6 us -> none  [combined_all(): gathered = jax.tree.map(lambda a: lax.all_gather(a, axis), part)]
    all_to_all x3 -> x0, starting transfers between devices: 12.1 us -> none  [the longest x1 4.19 us: per_device(): lax.all_to_all(total[None], 'tp', split_axis=2, concat_axis=0, tiled=True)]
    dot_general x14 -> x0, matrix products: 8.74 us -> none  [the longest x1 1.19 us: per_device(): out_part = jnp.dot(hidden, w_ff_out, preferred_element_type=f32)]
    convert_element_type x8 -> x0, other arithmetic: 3.48 us -> none  [the longest x1 0.77 us: rotate(): positions.astype(jnp.float32)[:, None, None] * inverse[None, None, :]]
    reshape x0 -> x4, local copies, waits for them, and re-layouts: none -> 2.27 us  [the longest x1 0.58 us: per_device_kernel(): gain_q.reshape(1, -1)]
  transfers between devices with their start and end apart: 4 -> 0, of which waited for: 1 -> 0; matrix products, arithmetic and copies ran while one was open for 2% -> 0% of each run, Pallas kernels for 0% -> 0%
where the time goes in v1:
time: 52 us; the launch traced here: 51.7 us
  Pallas kernels  45.2 us (87%)
  local copies, waits for them, and re-layouts  5.8 us (11%)
  between operations  0.66 us (1%)
    pallas_call x1, Pallas kernels, per_device_kernel(): pl.pallas_call(functools.partial(layer_kernel, n_kv, n_tp), out_shape=(ja...  45.2 us
    unnamed x15, local copies, waits for them, and re-layouts  3.53 us

profile of v1, /device:TPU:0, one launch (start us, length us, event | category | flops | bytes accessed | tf_op | source)
XLA Modules:
  0.0 51.7 jit_solution(18403075986191179468)
XLA Ops:
  0.6 0.0 copy-start.3
  0.6 0.6 %copy-done.3 = bf16[256]{0:T(256)(128)(2,1)S(1)} copy-done((bf16[256]{0:T(256)(128)(2,1)S(1)}, bf16[256]{0:T(256)(128)(2,1)}, u32[]{:S(2)}) %copy-start.3) | copy-done | bytes 536
  1.3 0.0 copy-start.4
  1.3 0.6 %reshape.27.gain_in = bf16[1,256]{1,0:T(2,128)(2,1)} reshape(bf16[256]{0:T(256)(128)(2,1)S(1)} %copy-done.3) | data formatting | bytes 1024 | tf_op jit(solution)/shard_map/reshape | solution.py:524
  1.9 0.1 copy-done.4
  1.9 0.0 copy-start.5
  1.9 0.6 %reshape.29.gain_kv = bf16[1,256]{1,0:T(2,128)(2,1)} reshape(bf16[256]{0:T(256)(128)(2,1)S(1)} %copy-done.4) | data formatting | bytes 1024 | tf_op jit(solution)/shard_map/reshape | solution.py:524
  2.5 0.1 copy-done.5
  2.6 0.0 copy-start.2
  2.6 0.6 %reshape.30.gain_mid = bf16[1,256]{1,0:T(2,128)(2,1)} reshape(bf16[256]{0:T(256)(128)(2,1)S(1)} %copy-done.5) | data formatting | bytes 1024 | tf_op jit(solution)/shard_map/reshape | solution.py:525
  3.2 0.1 copy-done.2
  3.3 0.6 %reshape.28.gain_q = bf16[1,512]{1,0:T(2,128)(2,1)} reshape(bf16[512]{0:T(512)(128)(2,1)S(1)} %copy-done.2) | data formatting | bytes 2048 | tf_op jit(solution)/shard_map/reshape | solution.py:524
  3.9 45.2 %layer.1 = (bf16[16,256]{1,0:T(8,128)(2,1)}, bf16[16,256]{1,0:T(8,128)(2,1)}, bf16[16,32]{1,0:T(8,128)(2,1)}) custom-call(bf16[16,256]{1,0:T(8,128)(2,1)} %tokens.1, s32[16]{0:T(128)} %lengths.1, bf16[1,256]{1,0:T(2,128)(2,1)} %reshape.27.gain_in, bf16[1,512]{1,0:T(2,128)(2,1)} %reshape.28.gain_q, bf16[1,256]{1,0:T(2,128)(2,1)} %reshape.29.gain_kv, ...), custom_call_target="tpu_custom_call" | custom-call | tf_op jit(solution)/shard_map/layer/pallas_call | solution.py:486
  49.1 0.0 copy-start
  49.1 1.3 %copy.24 = bf16[16,256]{1,0:T(8,128)(2,1)} copy(bf16[16,256]{1,0:T(8,128)(2,1)} %get-tuple-element.6) | data formatting | bytes 16384
  50.4 0.0 copy-done
  50.4 0.0 copy-start.1
  50.4 0.6 %copy.25 = bf16[16,256]{1,0:T(8,128)(2,1)} copy(bf16[16,256]{1,0:T(8,128)(2,1)S(1)} %copy-done) | data formatting | bytes 16384
  51.0 0.1 copy-done.1
  51.1 0.6 %copy.26 = bf16[16,32]{1,0:T(8,128)(2,1)} copy(bf16[16,32]{1,0:T(8,128)(2,1)S(1)} %copy-done.1) | data formatting | bytes 2048
Async XLA Ops:
  0.6 0.7 %copy-start.3 = (bf16[256]{0:T(256)(128)(2,1)S(1)}, bf16[256]{0:T(256)(128)(2,1)}, u32[]{:S(2)}) copy-start(bf16[256]{0:T(256)(128)(2,1)} %param.22) | copy-start | bytes 1540
  1.3 0.7 %copy-start.4 = (bf16[256]{0:T(256)(128)(2,1)S(1)}, bf16[256]{0:T(256)(128)(2,1)}, u32[]{:S(2)}) copy-start(bf16[256]{0:T(256)(128)(2,1)} %param.29) | copy-start | bytes 1540
  1.9 0.7 %copy-start.5 = (bf16[256]{0:T(256)(128)(2,1)S(1)}, bf16[256]{0:T(256)(128)(2,1)}, u32[]{:S(2)}) copy-start(bf16[256]{0:T(256)(128)(2,1)} %param.33) | copy-start | bytes 1540
  2.6 0.7 %copy-start.2 = (bf16[512]{0:T(512)(128)(2,1)S(1)}, bf16[512]{0:T(512)(128)(2,1)}, u32[]{:S(2)}) copy-start(bf16[512]{0:T(512)(128)(2,1)} %param.26) | copy-start | bytes 3076
  49.1 1.3 %copy-start = (bf16[16,256]{1,0:T(8,128)(2,1)S(1)}, bf16[16,256]{1,0:T(8,128)(2,1)}, u32[]{:S(2)}) copy-start(bf16[16,256]{1,0:T(8,128)(2,1)} %get-tuple-element.7) | copy-start | bytes 24580
  50.4 0.7 %copy-start.1 = (bf16[16,32]{1,0:T(8,128)(2,1)S(1)}, bf16[16,32]{1,0:T(8,128)(2,1)}, u32[]{:S(2)}) copy-start(bf16[16,32]{1,0:T(8,128)(2,1)} %get-tuple-element.8) | copy-start | bytes 3076

commit v2 on v1

--- a/solution.py
+++ b/solution.py
@@ -189,37 +189,39 @@
 
 def layer_kernel(
     n_kv, n_tp,
-    tokens, lengths, gain_in, gain_q, gain_kv, gain_mid,
+    tokens_h, gain_in_h, lengths_h, gain_q_h, gain_kv_h, gain_mid_h,
     latent_h, rope_h, down_q_h, down_kv_h, down_r_h, up_qn_h, up_qr_h, key_up_h, value_up_h,
     attn_out_h, ff_in_h, ff_out_h,
     mixed_ref, new_latent_ref, new_rope_ref,
+    tokens, gain_in, lengths, gain_q, gain_kv, gain_mid,
     latent, rope, down_q, down_kv, down_r, up_qn, up_qr, key_up, value_up, attn_out, ff_in, ff_out,
-    part_in, got_in, full_in, q_rows, r_rows, acc_rows, part_att, got_att, head_rows,
-    part_out, got_out, part_stat, got_stat, part_ff, got_ff, full_ff, part_mix, got_mix,
+    part_in, got_in, full_in, q_rows, r_rows, acc_rows, part_att, got_att, part_seq, got_seq,
+    head_rows, got_out, got_stat, part_ff, got_ff, full_ff, got_mix,
     load_sem, send_sem, recv_sem,
 ):
     f32 = jnp.float32
     bf16 = jnp.bfloat16
     kv = lax.axis_index("kv")
     tp = lax.axis_index("tp")
-    n_all = n_kv * n_tp
     me = kv * n_tp + tp
-    loads = []
-    for i, (src, dst) in enumerate((
-        (down_q_h, down_q), (down_kv_h, down_kv), (down_r_h, down_r), (up_qn_h, up_qn),
-        (up_qr_h, up_qr), (key_up_h, key_up), (latent_h, latent), (rope_h, rope),
-        (value_up_h, value_up), (attn_out_h, attn_out), (ff_in_h, ff_in), (ff_out_h, ff_out),
-    )):
-        copy = pltpu.make_async_copy(src, dst, load_sem.at[i])
+    loads = [
+        pltpu.make_async_copy(src, dst, load_sem.at[i])
+        for i, (src, dst) in enumerate((
+            (tokens_h, tokens), (gain_in_h, gain_in), (down_q_h, down_q), (down_kv_h, down_kv),
+            (down_r_h, down_r), (lengths_h, lengths), (gain_q_h, gain_q), (gain_kv_h, gain_kv),
+            (gain_mid_h, gain_mid), (up_qn_h, up_qn), (up_qr_h, up_qr), (key_up_h, key_up),
+            (latent_h, latent), (rope_h, rope), (value_up_h, value_up), (attn_out_h, attn_out),
+            (ff_in_h, ff_in), (ff_out_h, ff_out),
+        ))
+    ]
+    for copy in loads[:9]:
         copy.start()
-        loads.append(copy)
 
     barrier = pltpu.get_barrier_semaphore()
-    for d in range(1, n_all):
-        peer = lax.rem(me + d, n_all)
-        pl.semaphore_signal(
-            barrier, inc=1, device_id=(peer // n_tp, lax.rem(peer, n_tp)), device_id_type=MESH
-        )
+    peers = [(lax.rem(kv + d, n_kv), tp) for d in range(1, n_kv)]
+    peers += [(kv, lax.rem(tp + d, n_tp)) for d in range(1, n_tp)]
+    for peer in peers:
+        pl.semaphore_signal(barrier, inc=1, device_id=peer, device_id_type=MESH)
 
     def remote(src, dst, slot, where):
         return pltpu.make_async_remote_copy(
@@ -231,16 +233,12 @@
     slots = [0]
 
     def begin(axis, src_of, dst_of):
-        count, mine = {"kv": (n_kv, kv), "tp": (n_tp, tp), "all": (n_all, me)}[axis]
+        count, mine = {"kv": (n_kv, kv), "tp": (n_tp, tp)}[axis]
         base = slots[0]
         slots[0] += count - 1
 
         def where(index):
-            if axis == "kv":
-                return (index, tp)
-            if axis == "tp":
-                return (kv, index)
-            return (index // n_tp, lax.rem(index, n_tp))
+            return (index, tp) if axis == "kv" else (kv, index)
 
         arriving = []
         for d in range(1, count):
@@ -271,10 +269,15 @@
     scale = (nope + rope_size) ** (-0.5)
     d_model = width * n_kv
 
+    def wide(gain):
+        return gain[...].astype(f32)[None, :]
+
+    for copy in loads[:5]:
+        copy.wait()
+    for copy in loads[9:]:
+        copy.start()
     resid = tokens[...].astype(f32)
-    scaled_in = (resid * gain_in[...].astype(f32)).astype(bf16)
-    for copy in loads[:3]:
-        copy.wait()
+    scaled_in = (resid * wide(gain_in)).astype(bf16)
     square = jnp.sum(resid * resid, axis=1, keepdims=True)
     part = jnp.concatenate(
         [
@@ -289,10 +292,12 @@
     block = part.shape[1] // n_tp
     for i in range(n_tp):
         part_in[i] = part[:, i * block : (i + 1) * block]
-    pl.semaphore_wait(barrier, n_all - 1)
+    pl.semaphore_wait(barrier, len(peers))
     finish = begin("kv", lambda k: part_in.at[tp], lambda k: got_in.at[k])
     got_in[kv] = part_in[tp]
 
+    for copy in loads[5:9]:
+        copy.wait()
     lane = lax.broadcasted_iota(jnp.int32, (seqs, LANES), 1)
     row = lax.broadcasted_iota(jnp.int32, (seqs, LANES), 0)
     where_at = jnp.zeros((seqs, LANES), jnp.int32)
@@ -306,7 +311,7 @@
     finish()
     full_in[tp] = jnp.sum(got_in[...], axis=0)
     finish = begin("tp", lambda t: full_in.at[tp], lambda t: full_in.at[t])
-    for copy in loads[3:6]:
+    for copy in loads[9:12]:
         copy.wait()
     finish()
     sums = jnp.concatenate([full_in[i] for i in range(n_tp)], axis=1)
@@ -315,13 +320,13 @@
     query_latent = (
         lat_q
         * lax.rsqrt(jnp.mean(lat_q * lat_q, axis=1, keepdims=True) + EPS)
-        * gain_q[...].astype(f32)
+        * wide(gain_q)
     ).astype(bf16)
     lat_kv = inv_in * sums[:, q_rank : q_rank + kv_rank]
     new_latent = (
         lat_kv
         * lax.rsqrt(jnp.mean(lat_kv * lat_kv, axis=1, keepdims=True) + EPS)
-        * gain_kv[...].astype(f32)
+        * wide(gain_kv)
     ).astype(bf16)
     new_latent_ref[...] = new_latent
     new_latent = new_latent.astype(f32)
@@ -345,7 +350,7 @@
         ).astype(f32)
         r_rows[h] = query_rope[:, h * rope_size : (h + 1) * rope_size]
 
-    for copy in loads[6:9]:
+    for copy in loads[12:15]:
         copy.wait()
     first = me * rows
     at = first + lax.broadcasted_iota(jnp.int32, (heads, rows), 1)
@@ -392,13 +397,30 @@
             pieces.append(both[:seqs] + both[seqs:])
             stat = jnp.where(lane == i, acc[:, kv_rank : kv_rank + LANES], stat)
             stat = jnp.where(lane == own_heads + i, acc[:, kv_rank + LANES :], stat)
-        message = jnp.concatenate(pieces + [stat], axis=1)
-        for k in range(n_kv):
-            part_att[k * n_tp + t] = message[k * own_seqs : (k + 1) * own_seqs, :]
-    finish = begin("all", lambda p: part_att.at[p], lambda p: got_att.at[p])
-    got_att[me] = part_att[me]
-    finish()
-    got = got_att[...]
+        part_att[t] = jnp.concatenate(pieces + [stat], axis=1)
+    finish = begin("tp", lambda t: part_att.at[t], lambda t: got_att.at[t])
+    got_att[tp] = part_att[tp]
+    finish()
+
+    stats = [got_att[t][:, v_wide:] for t in range(n_tp)]
+    top = functools.reduce(jnp.maximum, stats)
+    head_lane = lax.broadcasted_iota(jnp.int32, (seqs, v_wide), 1) // v_size
+    joined = jnp.zeros((seqs, v_wide), f32)
+    totals = jnp.zeros((seqs, LANES), f32)
+    for t in range(n_tp):
+        fade_t = jnp.exp(stats[t] - top)
+        fade = jnp.zeros((seqs, v_wide), f32)
+        for i in range(own_heads):
+            fade = jnp.where(head_lane == i, fade_t[:, i : i + 1], fade)
+        joined += got_att[t][:, :v_wide] * fade
+        totals += stats[t] * pltpu.roll(fade_t, own_heads, 1)
+    message = jnp.concatenate([joined, jnp.where(lane < own_heads, top, totals)], axis=1)
+    for k in range(n_kv):
+        part_seq[k] = message[k * own_seqs : (k + 1) * own_seqs, :]
+    finish = begin("kv", lambda k: part_seq.at[k], lambda k: got_seq.at[k])
+    got_seq[kv] = part_seq[kv]
+    finish()
+    got = got_seq[...]
     values = got[:, :, :v_wide]
     stat = got[:, :, v_wide:]
     fade_all = jnp.exp(stat - jnp.max(stat, axis=0, keepdims=True))
@@ -413,20 +435,20 @@
         total = jnp.where(sum_lane == i, total_i, total)
     head_rows[kv] = (jnp.sum(values * fade, axis=0) / total).astype(bf16).astype(f32)
     finish = begin("kv", lambda k: head_rows.at[kv], lambda k: head_rows.at[k])
-    loads[9].wait()
+    loads[15].wait()
     finish()
     head_out = jnp.concatenate([head_rows[k] for k in range(n_kv)], axis=0).astype(bf16)
 
     got_out[tp] = dot_nn(head_out, attn_out[...])
     finish = begin("tp", lambda t: got_out.at[tp], lambda t: got_out.at[t])
-    loads[10].wait()
+    loads[16].wait()
     finish()
     resid_mid = resid + jnp.sum(got_out[...], axis=0)
     got_stat[kv] = jnp.broadcast_to(
         jnp.sum(resid_mid * resid_mid, axis=1, keepdims=True), (seqs, LANES)
     )
     finish_stat = begin("kv", lambda k: got_stat.at[kv], lambda k: got_stat.at[k])
-    scaled_mid = (resid_mid * gain_mid[...].astype(f32)).astype(bf16)
+    scaled_mid = (resid_mid * wide(gain_mid)).astype(bf16)
     hidden_part = dot_nn(scaled_mid, ff_in[...])
     piece = hidden_part.shape[1] // n_kv
     for k in range(n_kv):
@@ -435,7 +457,7 @@
     got_ff[kv] = part_ff[kv]
     finish_stat()
     inv_mid = lax.rsqrt(jnp.sum(got_stat[...], axis=0)[:, :1] / d_model + EPS)
-    loads[11].wait()
+    loads[17].wait()
     finish()
     full_ff[kv] = jnp.sum(got_ff[...], axis=0)
     finish = begin("kv", lambda k: full_ff.at[kv], lambda k: full_ff.at[k])
@@ -448,6 +470,12 @@
     mixed_ref[...] = (resid_mid + jnp.sum(got_mix[...], axis=0)).astype(bf16)
     for copy in sent:
         copy.wait_send()
+
+
+def hand_out(mixed, new_latent, new_rope, mixed_out, new_latent_out, new_rope_out):
+    mixed_out[...] = mixed[...]
+    new_latent_out[...] = new_latent[...]
+    new_rope_out[...] = new_rope[...]
 
 
 def per_device_kernel(
@@ -462,10 +490,15 @@
     kv_rank, _, v_size = w_value_up.shape
     rope_size = w_rope_key.shape[1]
     hidden = w_ff_in.shape[1]
-    n_all = n_kv * n_tp
     own_seqs = seqs // n_kv
     v_wide = heads // n_tp * v_size
     big = [
+        tokens,
+        gain_in,
+        lengths,
+        gain_q,
+        gain_kv,
+        gain_mid,
         latent_cache,
         rope_cache.transpose(0, 2, 1),
         w_down_q,
@@ -480,21 +513,21 @@
         w_ff_out,
     ]
     block = (q_rank + kv_rank + 2 * LANES) // n_tp
-    messages = 5 * (n_kv - 1) + 3 * (n_tp - 1) + (n_all - 1)
+    messages = 6 * (n_kv - 1) + 4 * (n_tp - 1)
     vmem = pltpu.VMEM
     whole = pl.BlockSpec(memory_space=pltpu.VMEM)
-    return pl.pallas_call(
+    results = pl.pallas_call(
         functools.partial(layer_kernel, n_kv, n_tp),
         out_shape=(
             jax.ShapeDtypeStruct((seqs, width), bf16),
             jax.ShapeDtypeStruct((seqs, kv_rank), bf16),
             jax.ShapeDtypeStruct((seqs, rope_size), bf16),
         ),
-        in_specs=[whole, pl.BlockSpec(memory_space=pltpu.SMEM)]
-        + [whole] * 4
-        + [pl.BlockSpec(memory_space=pl.ANY)] * len(big),
+        in_specs=[pl.BlockSpec(memory_space=pl.ANY)] * len(big),
         out_specs=(whole, whole, whole),
-        scratch_shapes=[vmem(a.shape, bf16) for a in big]
+        scratch_shapes=[
+            pltpu.SMEM(a.shape, a.dtype) if a is lengths else vmem(a.shape, a.dtype) for a in big
+        ]
         + [
             vmem((n_tp, seqs, block), f32),
             vmem((n_kv, seqs, block), f32),
@@ -502,17 +535,16 @@
             vmem((heads, seqs, kv_rank), f32),
             vmem((heads, seqs, rope_size), f32),
             vmem((seqs, heads, kv_rank + 2 * LANES), f32),
-            vmem((n_all, own_seqs, v_wide + LANES), f32),
-            vmem((n_all, own_seqs, v_wide + LANES), f32),
+            vmem((n_tp, seqs, v_wide + LANES), f32),
+            vmem((n_tp, seqs, v_wide + LANES), f32),
+            vmem((n_kv, own_seqs, v_wide + LANES), f32),
+            vmem((n_kv, own_seqs, v_wide + LANES), f32),
             vmem((n_kv, own_seqs, v_wide), f32),
-            vmem((8, LANES), f32),
             vmem((n_tp, seqs, width), f32),
-            vmem((8, LANES), f32),
             vmem((n_kv, seqs, LANES), f32),
             vmem((n_kv, seqs, hidden // n_kv), f32),
             vmem((n_kv, seqs, hidden // n_kv), f32),
             vmem((n_kv, seqs, hidden // n_kv), f32),
-            vmem((8, LANES), f32),
             vmem((n_tp, seqs, width), f32),
             pltpu.SemaphoreType.DMA((len(big),)),
             pltpu.SemaphoreType.DMA((messages,)),
@@ -520,10 +552,14 @@
         ],
         compiler_params=pltpu.CompilerParams(collective_id=0, has_side_effects=True),
         name="layer",
-    )(
-        tokens, lengths, gain_in.reshape(1, -1), gain_q.reshape(1, -1), gain_kv.reshape(1, -1),
-        gain_mid.reshape(1, -1), *big,
-    )
+    )(*big)
+    return pl.pallas_call(
+        hand_out,
+        out_shape=tuple(jax.ShapeDtypeStruct(a.shape, a.dtype) for a in results),
+        in_specs=[whole] * 3,
+        out_specs=(whole,) * 3,
+        name="hand_out",
+    )(*results)
 
 
 def kernel_fits(n_kv, n_tp, seqs, width, q_rank, kv_rank, rope_size, heads, v_size, hidden):

time: 52 us -> 46.9 us (0.902)
  local copies, waits for them, and re-layouts: 5.8 us -> 0 us
  Pallas kernels: 45.2 us -> 46 us
    unnamed x15 -> x0, local copies, waits for them, and re-layouts: 3.53 us -> none
    reshape x4 -> x0, local copies, waits for them, and re-layouts: 2.27 us -> none  [the longest x1 0.58 us: per_device_kernel(): gain_q.reshape(1, -1)]
    pallas_call x0 -> x1, Pallas kernels: none -> 1.32 us  [per_device_kernel(): pl.pallas_call(hand_out, out_shape=tuple((jax.ShapeDtypeStruct(a.shape, a...]
    pallas_call x1, Pallas kernels: 45.2 us -> 44.6 us  [per_device_kernel(): pl.pallas_call(functools.partial(layer_kernel, n_kv, n_tp), out_shape=(ja...]
where the time goes in v2:
time: 46.9 us; the launch traced here: 46.6 us
  Pallas kernels  46 us (98%)
  between operations  0.65 us (1%)
    pallas_call x1, Pallas kernels, per_device_kernel(): pl.pallas_call(functools.partial(layer_kernel, n_kv, n_tp), out_shape=(ja...  44.6 us
    pallas_call x1, Pallas kernels, per_device_kernel(): pl.pallas_call(hand_out, out_shape=tuple((jax.ShapeDtypeStruct(a.shape, a...  1.32 us

profile of v2, /device:TPU:0, one launch (start us, length us, event | category | flops | bytes accessed | tf_op | source)
XLA Modules:
  0.0 46.6 jit_solution(6217153945247756028)
XLA Ops:
  0.6 44.6 %layer.1 = (bf16[16,256]{1,0:T(8,128)(2,1)}, bf16[16,256]{1,0:T(8,128)(2,1)}, bf16[16,32]{1,0:T(8,128)(2,1)}) custom-call(bf16[16,256]{1,0:T(8,128)(2,1)} %tokens_h.1, bf16[256]{0:T(256)(128)(2,1)} %gain_in_h.1, s32[16]{0:T(128)} %lengths_h.1, bf16[512]{0:T(512)(128)(2,1)} %gain_q_h.1, bf16[256]{0:T(256)(128)(2,1)} %gain_kv_h.1, bf16[256]{0:T(256)(128)(2,1)} %gain_mid_h.1, ...), custom_call_target="tpu_custom_call" | custom-call | tf_op jit(solution)/shard_map/layer/pallas_call | solution.py:519
  45.3 1.3 %hand_out.1 = (bf16[16,256]{1,0:T(8,128)(2,1)}, bf16[16,256]{1,0:T(8,128)(2,1)}, bf16[16,32]{1,0:T(8,128)(2,1)}) custom-call(bf16[16,256]{1,0:T(8,128)(2,1)} %get-tuple-element.6.mixed, bf16[16,256]{1,0:T(8,128)(2,1)} %get-tuple-element.7.new_latent, bf16[16,32]{1,0:T(8,128)(2,1)} %get-tuple-element.8.new_rope), custom_call_target="tpu_custom_call" | custom-call | tf_op jit(solution)/shard_map/hand_out/pallas_call | solution.py:556

commit v3 on v2

--- a/solution.py
+++ b/solution.py
@@ -195,8 +195,8 @@
     mixed_ref, new_latent_ref, new_rope_ref,
     tokens, gain_in, lengths, gain_q, gain_kv, gain_mid,
     latent, rope, down_q, down_kv, down_r, up_qn, up_qr, key_up, value_up, attn_out, ff_in, ff_out,
-    part_in, got_in, full_in, q_rows, r_rows, acc_rows, part_att, got_att, part_seq, got_seq,
-    head_rows, got_out, got_stat, part_ff, got_ff, full_ff, got_mix,
+    part_in, got_in, full_in, q_rows, r_rows, acc_rows, part_att, got_att, got_top, got_seq,
+    got_out, got_stat, part_ff, got_ff, full_ff, got_mix,
     load_sem, send_sem, recv_sem,
 ):
     f32 = jnp.float32
@@ -232,7 +232,7 @@
     sent = []
     slots = [0]
 
-    def begin(axis, src_of, dst_of):
+    def begin(axis, src_of, dst_of, group=None, prepare=None):
         count, mine = {"kv": (n_kv, kv), "tp": (n_tp, tp)}[axis]
         base = slots[0]
         slots[0] += count - 1
@@ -241,17 +241,24 @@
             return (index, tp) if axis == "kv" else (kv, index)
 
         arriving = []
-        for d in range(1, count):
+        steps = sorted(range(1, count), key=lambda d: -min(d, count - d))
+        for i, d in enumerate(steps):
+            if prepare is not None and i % group == 0:
+                for ahead in steps[i : i + group]:
+                    prepare(lax.rem(mine + ahead, count))
             peer = lax.rem(mine + d, count)
             copy = remote(src_of(peer), dst_of(mine), base + d - 1, where(peer))
             copy.start()
             sent.append(copy)
             source = lax.rem(mine + count - d, count)
-            arriving.append(remote(dst_of(source), dst_of(source), base + d - 1, where(source)))
-
-        def finish():
-            for copy in arriving:
+            landed = remote(dst_of(source), dst_of(source), base + d - 1, where(source))
+            arriving.append((source, landed))
+
+        def finish(use=None):
+            for source, copy in reversed(arriving):
                 copy.wait_recv()
+                if use is not None:
+                    use(source)
 
         return finish
 
@@ -265,12 +272,15 @@
     v_size = value_up.shape[1]
     rows = latent.shape[1]
     own_heads = heads // n_tp
-    own_seqs = seqs // n_kv
     scale = (nope + rope_size) ** (-0.5)
     d_model = width * n_kv
 
     def wide(gain):
         return gain[...].astype(f32)[None, :]
+
+    def across(values):
+        spare = jnp.zeros((LANES - values.shape[0], LANES), f32)
+        return jnp.transpose(jnp.concatenate([values, spare], axis=0))
 
     for copy in loads[:5]:
         copy.wait()
@@ -414,30 +424,28 @@
             fade = jnp.where(head_lane == i, fade_t[:, i : i + 1], fade)
         joined += got_att[t][:, :v_wide] * fade
         totals += stats[t] * pltpu.roll(fade_t, own_heads, 1)
-    message = jnp.concatenate([joined, jnp.where(lane < own_heads, top, totals)], axis=1)
+    got_top[kv] = across(jnp.where(lane < own_heads, top, totals))[: got_top.shape[1], :]
+    got_seq[kv] = joined
+    finish_top = begin("kv", lambda k: got_top.at[kv], lambda k: got_top.at[k])
+    finish = begin("kv", lambda k: got_seq.at[kv], lambda k: got_seq.at[k])
+    loads[15].wait()
+    finish_top()
+    tops = [got_top[k][:own_heads, :] for k in range(n_kv)]
+    top = functools.reduce(jnp.maximum, tops)
+    fades = [jnp.exp(tops[k] - top) for k in range(n_kv)]
+    total = sum(got_top[k][own_heads : 2 * own_heads, :] * fades[k] for k in range(n_kv))
+    used = lax.broadcasted_iota(jnp.int32, total.shape, 1) < seqs
+    share = 1.0 / jnp.where(used, total, 1.0)
+    shares = across(jnp.concatenate([fade * share for fade in fades], axis=0))[:seqs, :]
+    finish()
+    head_sum = jnp.zeros((seqs, v_wide), f32)
     for k in range(n_kv):
-        part_seq[k] = message[k * own_seqs : (k + 1) * own_seqs, :]
-    finish = begin("kv", lambda k: part_seq.at[k], lambda k: got_seq.at[k])
-    got_seq[kv] = part_seq[kv]
-    finish()
-    got = got_seq[...]
-    values = got[:, :, :v_wide]
-    stat = got[:, :, v_wide:]
-    fade_all = jnp.exp(stat - jnp.max(stat, axis=0, keepdims=True))
-    head_lane = lax.broadcasted_iota(jnp.int32, values.shape, 2) // v_size
-    sum_lane = lax.broadcasted_iota(jnp.int32, (own_seqs, v_wide), 1) // v_size
-    fade = jnp.zeros(values.shape, f32)
-    total = jnp.ones((own_seqs, v_wide), f32)
-    for i in range(own_heads):
-        fade_i = fade_all[:, :, i : i + 1]
-        total_i = jnp.sum(stat[:, :, own_heads + i : own_heads + i + 1] * fade_i, axis=0)
-        fade = jnp.where(head_lane == i, fade_i, fade)
-        total = jnp.where(sum_lane == i, total_i, total)
-    head_rows[kv] = (jnp.sum(values * fade, axis=0) / total).astype(bf16).astype(f32)
-    finish = begin("kv", lambda k: head_rows.at[kv], lambda k: head_rows.at[k])
-    loads[15].wait()
-    finish()
-    head_out = jnp.concatenate([head_rows[k] for k in range(n_kv)], axis=0).astype(bf16)
+        fade = jnp.zeros((seqs, v_wide), f32)
+        for i in range(own_heads):
+            at_lane = k * own_heads + i
+            fade = jnp.where(head_lane == i, shares[:, at_lane : at_lane + 1], fade)
+        head_sum += got_seq[k] * fade
+    head_out = head_sum.astype(bf16)
 
     got_out[tp] = dot_nn(head_out, attn_out[...])
     finish = begin("tp", lambda t: got_out.at[tp], lambda t: got_out.at[t])
@@ -449,22 +457,33 @@
     )
     finish_stat = begin("kv", lambda k: got_stat.at[kv], lambda k: got_stat.at[k])
     scaled_mid = (resid_mid * wide(gain_mid)).astype(bf16)
-    hidden_part = dot_nn(scaled_mid, ff_in[...])
-    piece = hidden_part.shape[1] // n_kv
-    for k in range(n_kv):
-        part_ff[k] = hidden_part[:, k * piece : (k + 1) * piece]
-    finish = begin("kv", lambda k: part_ff.at[k], lambda k: got_ff.at[k])
-    got_ff[kv] = part_ff[kv]
+    piece = ff_in.shape[1] // n_kv
+
+    def hidden_of(k):
+        columns = pl.ds(pl.multiple_of(k * piece, LANES), piece)
+        return dot_nn(scaled_mid, ff_in[:, columns])
+
+    def prepare(k):
+        part_ff[k] = hidden_of(k)
+
+    finish = begin("kv", lambda k: part_ff.at[k], lambda k: got_ff.at[k], n_kv // 2, prepare)
+    got_ff[kv] = hidden_of(kv)
     finish_stat()
     inv_mid = lax.rsqrt(jnp.sum(got_stat[...], axis=0)[:, :1] / d_model + EPS)
     loads[17].wait()
     finish()
     full_ff[kv] = jnp.sum(got_ff[...], axis=0)
     finish = begin("kv", lambda k: full_ff.at[kv], lambda k: full_ff.at[k])
-    finish()
-    hidden_sum = jnp.concatenate([full_ff[k] for k in range(n_kv)], axis=1)
-    hidden = jnp.square(jnp.maximum(inv_mid * hidden_sum, 0.0)).astype(bf16)
-    got_mix[tp] = dot_nn(hidden, ff_out[...])
+    out_parts = []
+
+    def use(k):
+        hidden = jnp.square(jnp.maximum(inv_mid * full_ff[k], 0.0)).astype(bf16)
+        columns = pl.ds(pl.multiple_of(k * piece, LANES), piece)
+        out_parts.append(dot_nn(hidden, ff_out[columns, :]))
+
+    use(kv)
+    finish(use)
+    got_mix[tp] = sum(out_parts)
     finish = begin("tp", lambda t: got_mix.at[tp], lambda t: got_mix.at[t])
     finish()
     mixed_ref[...] = (resid_mid + jnp.sum(got_mix[...], axis=0)).astype(bf16)
@@ -490,8 +509,8 @@
     kv_rank, _, v_size = w_value_up.shape
     rope_size = w_rope_key.shape[1]
     hidden = w_ff_in.shape[1]
-    own_seqs = seqs // n_kv
     v_wide = heads // n_tp * v_size
+    top_rows = pl.cdiv(2 * (heads // n_tp), 8) * 8
     big = [
         tokens,
         gain_in,
@@ -537,9 +556,8 @@
             vmem((seqs, heads, kv_rank + 2 * LANES), f32),
             vmem((n_tp, seqs, v_wide + LANES), f32),
             vmem((n_tp, seqs, v_wide + LANES), f32),
-            vmem((n_kv, own_seqs, v_wide + LANES), f32),
-            vmem((n_kv, own_seqs, v_wide + LANES), f32),
-            vmem((n_kv, own_seqs, v_wide), f32),
+            vmem((n_kv, top_rows, LANES), f32),
+            vmem((n_kv, seqs, v_wide), f32),
             vmem((n_tp, seqs, width), f32),
             vmem((n_kv, seqs, LANES), f32),
             vmem((n_kv, seqs, hidden // n_kv), f32),
@@ -564,8 +582,9 @@
 
 def kernel_fits(n_kv, n_tp, seqs, width, q_rank, kv_rank, rope_size, heads, v_size, hidden):
     return (
-        seqs % n_kv == 0
-        and heads % n_tp == 0
+        heads % n_tp == 0
+        and seqs <= LANES
+        and n_kv * (heads // n_tp) <= LANES
         and width % LANES == 0
         and q_rank % LANES == 0
         and kv_rank % LANES == 0

time: 46.9 us -> 45.1 us (0.962)
  Pallas kernels: 46 us -> 44.2 us
    pallas_call x1, Pallas kernels: 44.6 us -> 42.8 us  [per_device_kernel(): pl.pallas_call(functools.partial(layer_kernel, n_kv, n_tp), out_shape=(ja...]
where the time goes in v3:
time: 45.1 us; the launch traced here: 44.8 us
  Pallas kernels  44.2 us (98%)
  between operations  0.65 us (1%)
    pallas_call x1, Pallas kernels, per_device_kernel(): pl.pallas_call(functools.partial(layer_kernel, n_kv, n_tp), out_shape=(ja...  42.8 us
    pallas_call x1, Pallas kernels, per_device_kernel(): pl.pallas_call(hand_out, out_shape=tuple((jax.ShapeDtypeStruct(a.shape, a...  1.32 us

profile of v3, /device:TPU:0, one launch (start us, length us, event | category | flops | bytes accessed | tf_op | source)
XLA Modules:
  0.0 44.8 jit_solution(15421707130076799765)
XLA Ops:
  0.6 42.8 %layer.1 = (bf16[16,256]{1,0:T(8,128)(2,1)}, bf16[16,256]{1,0:T(8,128)(2,1)}, bf16[16,32]{1,0:T(8,128)(2,1)}) custom-call(bf16[16,256]{1,0:T(8,128)(2,1)} %tokens_h.1, bf16[256]{0:T(256)(128)(2,1)} %gain_in_h.1, s32[16]{0:T(128)} %lengths_h.1, bf16[512]{0:T(512)(128)(2,1)} %gain_q_h.1, bf16[256]{0:T(256)(128)(2,1)} %gain_kv_h.1, bf16[256]{0:T(256)(128)(2,1)} %gain_mid_h.1, ...), custom_call_target="tpu_custom_call" | custom-call | tf_op jit(solution)/shard_map/layer/pallas_call | solution.py:538
  43.5 1.3 %hand_out.1 = (bf16[16,256]{1,0:T(8,128)(2,1)}, bf16[16,256]{1,0:T(8,128)(2,1)}, bf16[16,32]{1,0:T(8,128)(2,1)}) custom-call(bf16[16,256]{1,0:T(8,128)(2,1)} %get-tuple-element.6.mixed, bf16[16,256]{1,0:T(8,128)(2,1)} %get-tuple-element.7.new_latent, bf16[16,32]{1,0:T(8,128)(2,1)} %get-tuple-element.8.new_rope), custom_call_target="tpu_custom_call" | custom-call | tf_op jit(solution)/shard_map/hand_out/pallas_call | solution.py:574

commit v4 on v3

--- a/solution.py
+++ b/solution.py
@@ -538,9 +538,9 @@
     results = pl.pallas_call(
         functools.partial(layer_kernel, n_kv, n_tp),
         out_shape=(
-            jax.ShapeDtypeStruct((seqs, width), bf16),
-            jax.ShapeDtypeStruct((seqs, kv_rank), bf16),
-            jax.ShapeDtypeStruct((seqs, rope_size), bf16),
+            pltpu.VMEM((seqs, width), bf16),
+            pltpu.VMEM((seqs, kv_rank), bf16),
+            pltpu.VMEM((seqs, rope_size), bf16),
         ),
         in_specs=[pl.BlockSpec(memory_space=pl.ANY)] * len(big),
         out_specs=(whole, whole, whole),
@@ -577,7 +577,7 @@
         in_specs=[whole] * 3,
         out_specs=(whole,) * 3,
         name="hand_out",
-    )(*results)
+    )(*(pltpu.with_memory_space_constraint(a, pltpu.VMEM) for a in results))
 
 
 def kernel_fits(n_kv, n_tp, seqs, width, q_rank, kv_rank, rope_size, heads, v_size, hidden):

time: 45.1 us -> 43.7 us (0.969)
  Pallas kernels: 44.2 us -> 42.8 us
    pallas_call x1, Pallas kernels: 1.32 us -> 0.61 us  [per_device_kernel(): pl.pallas_call(hand_out, out_shape=tuple((jax.ShapeDtypeStruct(a.shape, a...]
    pallas_call x1, Pallas kernels: 42.8 us -> 42.2 us  [per_device_kernel(): pl.pallas_call(functools.partial(layer_kernel, n_kv, n_tp), out_shape=(pl...]
where the time goes in v4:
time: 43.7 us; the launch traced here: 43.5 us
  Pallas kernels  42.8 us (98%)
  between operations  0.65 us (1%)
    pallas_call x1, Pallas kernels, per_device_kernel(): pl.pallas_call(functools.partial(layer_kernel, n_kv, n_tp), out_shape=(pl...  42.2 us

profile of v4, /device:TPU:0, one launch (start us, length us, event | category | flops | bytes accessed | tf_op | source)
XLA Modules:
  0.0 43.5 jit_solution(15825095331033798501)
XLA Ops:
  0.6 42.2 %layer.1 = (bf16[16,256]{1,0:T(8,128)(2,1)S(1)}, bf16[16,256]{1,0:T(8,128)(2,1)S(1)}, bf16[16,32]{1,0:T(8,128)(2,1)S(1)}) custom-call(bf16[16,256]{1,0:T(8,128)(2,1)} %tokens_h.1, bf16[256]{0:T(256)(128)(2,1)} %gain_in_h.1, s32[16]{0:T(128)} %lengths_h.1, bf16[512]{0:T(512)(128)(2,1)} %gain_q_h.1, bf16[256]{0:T(256)(128)(2,1)} %gain_kv_h.1, ...), custom_call_target="tpu_custom_call" | custom-call | tf_op jit(solution)/shard_map/layer/pallas_call | solution.py:538
  42.9 0.6 %hand_out.1 = (bf16[16,256]{1,0:T(8,128)(2,1)}, bf16[16,256]{1,0:T(8,128)(2,1)}, bf16[16,32]{1,0:T(8,128)(2,1)}) custom-call(bf16[16,256]{1,0:T(8,128)(2,1)S(1)} %get-tuple-element.6.mixed, bf16[16,256]{1,0:T(8,128)(2,1)S(1)} %get-tuple-element.7.new_latent, bf16[16,32]{1,0:T(8,128)(2,1)S(1)} %get-tuple-element.8.new_rope), custom_call_target="tpu_custom_call" | custom-call | tf_op jit(solution)/shard_map/hand_out/pallas_call | solution.py:574
